TPU v7x, 256 devices: a 4x2x16 block of a 4x16x16 slice. The times are simulated.
256 devices in a mesh: grp: 2 (over y), sp: 16 (over z), tp: 8 (over x, core).
Axes of the slice: x: 4, y: 2, z: 16, core: 2. Of those that a mesh axis runs over, the one named last changes fastest.
The devices are a block of a 4x16x16 slice.
Arguments:
- tokens: bfloat16 [8192, 8, 2048], P('sp', 'grp'), parts along dimension 1, may hold values from -48 to 48
- query_weight: bfloat16 [2048, 1024], P(None, 'tp'), may hold values from -2 to 2
- key_weight: bfloat16 [2048, 1024], P(None, 'tp'), may hold values from -2 to 2
- value_weight: bfloat16 [2048, 1024], P(None, 'tp'), may hold values from -3 to 3
- mix_gain: float32 [1024], P('tp'), may hold values from 0.1 to 1.9
- out_weight: bfloat16 [1024, 2048], P('tp'), may hold values from -0.1875 to 0.1875
Outputs:
- mixed: bfloat16 [8192, 8, 2048], P(('sp', 'tp'), 'grp'), parts along dimension 1
There are 2 independent parts, one for each index of `grp`. A program takes and returns all parts, laid end to end along the dimension named above; an argument that names none is the same for every part. Nothing has to cross between parts.
All inputs are finite; a program needn't handle non-finite values.
Results may differ from a plain program's by a relative error of at most 0.02.
Values may be sent and summed in bfloat16 or wider, within the bound.
A program may use at most 128 MiB of HBM per device.

v0:
```python
import functools

import jax
import jax.numpy as jnp
from jax import lax
from jax.experimental import pallas as pl
from jax.experimental.pallas import tpu as pltpu
from jax.sharding import PartitionSpec as P

HEAD_DIM = 64
LANES = 128
CLASSES = 4
EPSILON = 1e-06
NEGATIVE = -1e30
BF = jnp.bfloat16
F32 = jnp.float32
MESH_ID = pl.DeviceIdType.MESH


def kernel(
    n_sp, n_tp,
    tokens, wq, wk, wv, gain, wo,
    out,
    tok, wqkv, wall, gall, acc, q_own, kv_own, kv_prev, q_two, q_three,
    o_three, s_three, i_three, t_three, o_two, s_two, i_two, t_two,
    n_loc, s_loc, corner_v, bias0, bias1, biasc, bias2, bias4,
    x_send, x_recv, x_rows,
    tok_sem, w_sem, own_sem,
    q_ss, q_rs, f_ss, f_rs, k_ss, k_rs,
    o3_ss, o3_rs, t3_ss, t3_rs, o2_ss, o2_rs, t2_ss, t2_rs,
    x_ss, x_rs, g_ss, g_rs, w_ss, w_rs, v_ss, v_rs,
):
    batch = tok.shape[2]
    size = tok.shape[1]
    share = size // n_tp
    reach = size // CLASSES
    z = lax.axis_index("sp")
    me = lax.axis_index("tp")

    def along(step):
        return lax.rem(z + step + n_sp, n_sp)

    def peer(step):
        return lax.rem(me + step, n_tp)

    sibling = me + 1 - 2 * lax.rem(me, 2)

    def remote(src, dst, send, recv, axis, where):
        return pltpu.make_async_remote_copy(
            src_ref=src, dst_ref=dst, send_sem=send, recv_sem=recv,
            device_id={axis: where}, device_id_type=MESH_ID,
        )

    def tok_copy(c):
        return pltpu.make_async_copy(tokens.at[:, c], tok.at[c], tok_sem.at[c])

    weights = [
        pltpu.make_async_copy(w, wqkv.at[:, pl.ds(i * LANES, LANES)], w_sem.at[i])
        for i, w in enumerate((wq, wk, wv))
    ]
    for copy in weights:
        copy.start()
    for c in range(CLASSES):
        tok_copy(c).start()
    own_w = pltpu.make_async_copy(wo, wall.at[me], own_sem)
    own_w.start()
    gall[pl.ds(me, 1)] = gain[...][None]

    barrier = pltpu.get_barrier_semaphore()
    for step in (-2, -1, 1, 2):
        pl.semaphore_signal(barrier, inc=1, device_id={"sp": along(step)}, device_id_type=MESH_ID)
    for step in range(1, n_tp):
        pl.semaphore_signal(barrier, inc=1, device_id={"tp": peer(step)}, device_id_type=MESH_ID)

    key = lax.broadcasted_iota(jnp.int32, (size, LANES), 0)
    query = lax.broadcasted_iota(jnp.int32, (size, LANES), 1)

    def log_count(count):
        return jnp.where(
            count == 0, NEGATIVE,
            jnp.where(count == 1, 0.0, jnp.where(count == 2, 0.6931471805599453, 1.0986122886681098)),
        ).astype(F32)

    for diff in range(1 - CLASSES, CLASSES):
        gap = CLASSES * (query - key) + diff
        count = ((gap >= 0) & (gap <= 128)).astype(jnp.int32)
        if diff == 0:
            count = count + ((gap >= 0) & (gap <= 512)).astype(jnp.int32)
            count = count + ((gap >= 0) & (((query - key) & 3) == 0)).astype(jnp.int32)
        bias0[diff + CLASSES - 1] = log_count(count)
    same = (((query - key) & 3) == 0).astype(jnp.int32)
    bias1[...] = log_count((key >= query).astype(jnp.int32) + same)
    bias2[...] = log_count(same)
    bias4[...] = log_count(jnp.where(key >= query, same, 0)) + jnp.where(z >= 1, 0.0, NEGATIVE)
    for c in range(CLASSES):
        gap = CLASSES * size + CLASSES * (query - (size - reach + lax.rem(key, reach))) + c - key // reach
        biasc[c] = log_count((gap <= 128).astype(jnp.int32))

    pl.semaphore_wait(barrier, 4 + n_tp - 1)

    gains = [
        remote(gall.at[me], gall.at[me], g_ss.at[j - 1], g_rs.at[j - 1], "tp", peer(j))
        for j in range(1, n_tp)
    ]
    across = [
        remote(wo, wall.at[me], w_ss.at[j // 2 - 1], w_rs.at[j // 2 - 1], "tp", peer(j))
        for j in range(2, n_tp, 2)
    ]
    for copy in gains + across:
        copy.start()
    beside = [remote(wo, wall.at[me], v_ss.at[0], v_rs.at[0], "tp", sibling)]
    beside[0].start()

    def send_q(c):
        return remote(q_own.at[c], q_two.at[c], q_ss.at[c], q_rs.at[c], "sp", along(-2))

    def pass_q(c):
        return remote(q_two.at[c], q_three.at[c], f_ss.at[c], f_rs.at[c], "sp", along(-1))

    def send_kv(c):
        return remote(kv_own.at[c], kv_prev.at[c], k_ss.at[c], k_rs.at[c], "sp", along(1))

    def send_three(c):
        return (
            remote(o_three.at[c], i_three.at[c], o3_ss.at[c], o3_rs.at[c], "sp", along(1)),
            remote(s_three.at[c], t_three.at[c], t3_ss.at[c], t3_rs.at[c], "sp", along(1)),
        )

    def send_two(c):
        return (
            remote(o_two.at[c], i_two.at[c], o2_ss.at[c], o2_rs.at[c], "sp", along(2)),
            remote(s_two.at[c], t_two.at[c], t2_ss.at[c], t2_rs.at[c], "sp", along(2)),
        )

    for copy in weights:
        copy.wait()

    @pl.loop(0, CLASSES)
    def _(c):
        tok_copy(c).wait()
        rows = tok[c].reshape(size * batch, tok.shape[3])
        product = jnp.dot(rows, wqkv[...], preferred_element_type=F32)
        for i in range(3):
            acc[i] = product[:, i * LANES:(i + 1) * LANES]
        for b in range(batch):
            picked = pl.ds(b, size, stride=batch)
            q_own[c, b] = (acc[0, picked, :] * HEAD_DIM ** (-0.5)).astype(BF)
            kv_own[c, b, 0] = acc[1, picked, :].astype(BF)
            kv_own[c, b, 1] = acc[2, picked, :].T.astype(BF)
        send_q(c).start()
        send_kv(c).start()

    lane = lax.broadcasted_iota(jnp.int32, (1, LANES), 1)
    head0 = jnp.where(lane < HEAD_DIM, 1.0, 0.0).astype(BF)
    head1 = jnp.where(lane < HEAD_DIM, 0.0, 1.0).astype(BF)

    def attend(query_rows, keys, values, bias):
        count = keys.shape[0]
        both = jnp.concatenate([keys * head0, keys * head1], axis=0)
        scores = lax.dot_general(
            both, query_rows, (((1,), (1,)), ((), ())), preferred_element_type=F32
        )
        state = []
        for h in range(2):
            score = scores[h * count:(h + 1) * count] + bias
            top = jnp.max(score, axis=0, keepdims=True)
            raised = jnp.exp(score - top)
            total = jnp.sum(raised, axis=0, keepdims=True)
            part = jnp.dot(
                values[h * HEAD_DIM:(h + 1) * HEAD_DIM], raised.astype(BF),
                preferred_element_type=F32,
            )
            state.append((part, top, total))
        return state

    def merge(one, two):
        merged = []
        for (part_a, top_a, total_a), (part_b, top_b, total_b) in zip(one, two):
            top = jnp.maximum(top_a, top_b)
            by_a, by_b = jnp.exp(top_a - top), jnp.exp(top_b - top)
            merged.append((part_a * by_a + part_b * by_b, top, total_a * by_a + total_b * by_b))
        return merged

    def masked(state, valid):
        return [(part, jnp.where(valid, top, NEGATIVE), total) for part, top, total in state]

    def put(part_ref, stat_ref, c, b, state):
        for h in range(2):
            part, top, total = state[h]
            part_ref[c, b, h * HEAD_DIM:(h + 1) * HEAD_DIM, :] = part.astype(part_ref.dtype)
            stat_ref[c, b, h:h + 1, :] = top
            stat_ref[c, b, 2 + h:3 + h, :] = total

    def get(part_ref, stat_ref, c, b):
        return [
            (
                part_ref[c, b, h * HEAD_DIM:(h + 1) * HEAD_DIM, :].astype(F32),
                stat_ref[c, b, h:h + 1, :],
                stat_ref[c, b, 2 + h:3 + h, :],
            )
            for h in range(2)
        ]

    @pl.loop(0, CLASSES)
    def _(c):
        send_q(c).wait_recv()
        pass_q(c).start()

        @pl.loop(0, batch)
        def _(b):
            keys = jnp.concatenate([kv_own[j, b, 0] for j in range(CLASSES)], axis=0)
            values = jnp.concatenate([kv_own[j, b, 1] for j in range(CLASSES)], axis=1)
            bias = jnp.concatenate([bias0[c - j + CLASSES - 1] for j in range(CLASSES)], axis=0)
            put(n_loc, s_loc, c, b, attend(q_own[c, b], keys, values, bias))

    @pl.loop(0, CLASSES)
    def _(c):
        pass_q(c).wait_recv()
        send_kv(c).wait_recv()
        bias = jnp.concatenate([bias2[...], bias4[...]], axis=0)
        for b in range(batch):
            keys = jnp.concatenate([kv_own[c, b, 0], kv_prev[c, b, 0]], axis=0)
            values = jnp.concatenate([kv_own[c, b, 1], kv_prev[c, b, 1]], axis=1)
            state = masked(attend(q_three[c, b], keys, values, bias), z + 3 < n_sp)
            put(o_three, s_three, c, b, state)
        for copy in send_three(c):
            copy.start()

    @pl.loop(0, CLASSES)
    def _(c):
        for copy in send_three(c):
            copy.wait_recv()
        for b in range(batch):
            state = masked(
                attend(q_two[c, b], kv_own[c, b, 0], kv_own[c, b, 1], bias2[...]), z + 2 < n_sp
            )
            put(o_two, s_two, c, b, merge(state, get(i_three, t_three, c, b)))
        for copy in send_two(c):
            copy.start()

    pick_row = lax.broadcasted_iota(jnp.int32, (LANES, LANES), 0)
    pick_col = lax.broadcasted_iota(jnp.int32, (LANES, LANES), 1)

    @pl.loop(0, batch)
    def _(b):
        gathered = jnp.zeros((LANES, LANES), F32)
        for j in range(CLASSES):
            hot = (pick_row == size - reach + pick_col - j * reach) & (pick_col // reach == j)
            gathered = gathered + jnp.dot(
                kv_prev[j, b, 1], jnp.where(hot, 1.0, 0.0).astype(BF), preferred_element_type=F32
            )
        corner_v[b] = gathered.astype(BF)

    @pl.loop(0, CLASSES)
    def _(c):
        bias = jnp.concatenate([bias1[...], biasc[c]], axis=0)
        for b in range(batch):
            keys = jnp.concatenate(
                [kv_prev[c, b, 0]]
                + [kv_prev[j, b, 0, size - reach:size, :] for j in range(CLASSES)], axis=0
            )
            values = jnp.concatenate([kv_prev[c, b, 1], corner_v[b]], axis=1)
            state = masked(attend(q_own[c, b], keys, values, bias), z >= 1)
            put(n_loc, s_loc, c, b, merge(state, get(n_loc, s_loc, c, b)))

    for j, copy in enumerate(across):
        copy.wait_recv()
        block = wall.at[peer(n_tp - 2 * (j + 1))]
        beside.append(remote(block, block, v_ss.at[j + 1], v_rs.at[j + 1], "tp", sibling))
        beside[-1].start()

    def send_x(c, j):
        to = peer(j)
        rows = pl.ds(pl.multiple_of(to * share, share), share)
        return remote(
            x_send.at[c, :, rows, :], x_recv.at[c, me], x_ss.at[c, j - 1], x_rs.at[c, j - 1],
            "tp", to,
        )

    def finish(c):
        for copy in send_two(c):
            copy.wait_recv()
        for b in range(batch):
            state = merge(get(n_loc, s_loc, c, b), get(i_two, t_two, c, b))
            mixed = jnp.concatenate([part / total for part, _, total in state], axis=0)
            x_send[c, b] = mixed.T.astype(BF)
        for j in range(1, n_tp):
            send_x(c, j).start()
        for b in range(batch):
            x_recv[c, me, b] = x_send[c, b, pl.ds(pl.multiple_of(me * share, share), share), :]

    def project(c):
        for j in range(1, n_tp):
            send_x(c, j).wait_recv()
        squares = jnp.zeros((share * batch, LANES), F32)
        for r in range(n_tp):
            for b in range(batch):
                x_rows[r, pl.ds(b, share, stride=batch), :] = x_recv[c, r, b].astype(F32)
            squares = squares + x_rows[r] * x_rows[r]
        mean = jnp.sum(squares, axis=1, keepdims=True) / (n_tp * LANES)
        scale = lax.rsqrt(mean + EPSILON)
        normed = jnp.concatenate(
            [(x_rows[r] * scale * gall[r]).astype(BF) for r in range(n_tp)], axis=1
        )
        width = out.shape[3]
        step = min(512, width)
        for at in range(0, width, step):
            weight = wall[:, :, at:at + step].reshape(n_tp * LANES, step)
            block = jnp.dot(normed, weight, preferred_element_type=F32).astype(BF)
            out[:, c, :, at:at + step] = block.reshape(share, batch, step)

    finish(0)
    own_w.wait()
    for copy in gains:
        copy.wait_recv()
    for copy in beside:
        copy.wait_recv()

    @pl.loop(1, CLASSES)
    def _(c):
        finish(c)
        project(c - 1)

    project(CLASSES - 1)

    for copy in gains + across + beside:
        copy.wait_send()

    @pl.loop(0, CLASSES)
    def _(c):
        for copy in (send_q(c), pass_q(c), send_kv(c)) + send_three(c) + send_two(c):
            copy.wait_send()
        for j in range(1, n_tp):
            send_x(c, j).wait_send()


def body(n_sp, n_tp, tokens, wq, wk, wv, gain, wo):
    rows, batch, width = tokens.shape
    size = rows // CLASSES
    share = size // n_tp
    tokens = tokens.reshape(size, CLASSES, batch, width)
    any_spec = pl.BlockSpec(memory_space=pl.ANY)
    vmem_spec = pl.BlockSpec(memory_space=pltpu.VMEM)
    blocks = (CLASSES, batch, LANES, LANES)
    stats = (CLASSES, batch, 4, LANES)
    dma = pltpu.SemaphoreType.DMA
    tiles = pltpu.VMEM((LANES, LANES), F32)
    scratch = (
        [
            pltpu.VMEM((CLASSES, size, batch, width), BF),
            pltpu.VMEM((width, 3 * LANES), BF),
            pltpu.VMEM((n_tp, LANES, wo.shape[1]), BF),
            pltpu.VMEM((n_tp, 1, LANES), F32),
            pltpu.VMEM((3, size * batch, LANES), F32),
            pltpu.VMEM(blocks, BF),
            pltpu.VMEM((CLASSES, batch, 2, LANES, LANES), BF),
            pltpu.VMEM((CLASSES, batch, 2, LANES, LANES), BF),
            pltpu.VMEM(blocks, BF),
            pltpu.VMEM(blocks, BF),
        ]
        + [pltpu.VMEM(blocks, BF), pltpu.VMEM(stats, F32)] * 4
        + [
            pltpu.VMEM(blocks, F32),
            pltpu.VMEM(stats, F32),
            pltpu.VMEM((batch, LANES, LANES), BF),
            pltpu.VMEM((2 * CLASSES - 1, LANES, LANES), F32),
            tiles,
            pltpu.VMEM((CLASSES, LANES, LANES), F32),
            tiles,
            tiles,
            pltpu.VMEM(blocks, BF),
            pltpu.VMEM((CLASSES, n_tp, batch, share, LANES), BF),
            pltpu.VMEM((n_tp, share * batch, LANES), F32),
            dma((CLASSES,)),
            dma((3,)),
            dma(()),
        ]
        + [dma((CLASSES,))] * 14
        + [dma((CLASSES, n_tp - 1))] * 2
        + [dma((n_tp - 1,))] * 2
        + [dma((n_tp // 2 - 1,))] * 2
        + [dma((n_tp // 2,))] * 2
    )
    result = pl.pallas_call(
        functools.partial(kernel, n_sp, n_tp),
        out_shape=jax.ShapeDtypeStruct((share, CLASSES, batch, width), BF),
        in_specs=[any_spec] * 4 + [vmem_spec, any_spec],
        out_specs=vmem_spec,
        scratch_shapes=scratch,
        compiler_params=pltpu.CompilerParams(
            collective_id=0, has_side_effects=True, vmem_limit_bytes=60 * 1024 * 1024
        ),
        name="attend_all",
    )(tokens, wq, wk, wv, gain.reshape(1, LANES), wo)
    return result.reshape(share * CLASSES, batch, width)


def solution(mesh):
    in_specs = (
        P("sp", "grp", None),
        P(None, "tp"),
        P(None, "tp"),
        P(None, "tp"),
        P("tp"),
        P("tp", None),
    )
    out_specs = P(("sp", "tp"), "grp", None)
    step = functools.partial(body, mesh.shape["sp"], mesh.shape["tp"])
    return jax.shard_map(step, mesh=mesh, in_specs=in_specs, out_specs=out_specs, check_vma=False)
```

profile of v0, /device:TPU:33, one launch (start us, length us, event | category | flops | bytes accessed | tf_op | source)
XLA Modules:
  0.0 104.5 jit_solution(11749043449822338774)
XLA Ops:
  0.0 101.8 %attend_all.1 = bf16[16,4,4,2048]{3,2,1,0:T(4,128)(2,1)} custom-call(bf16[128,4,4,2048]{3,2,1,0:T(4,128)(2,1)} %bitcast.3, bf16[2048,128]{1,0:T(8,128)(2,1)} %wq.1, bf16[2048,128]{1,0:T(8,128)(2,1)} %wk.1, bf16[2048,128]{1,0:T(8,128)(2,1)} %wv.1, f32[1,128]{1,0:T(1,128)} %bitcast.5, bf16[128,2048]{1,0:T(8,128)(2,1)} %wo.1), custom_call_target="tpu_custom_call" | custom-call | tf_op jit(solution)/shard_map/attend_all/pallas_call | solution.py:384
  101.8 2.7 %copy.8 = bf16[64,4,2048]{2,1,0:T(4,128)(2,1)} copy(bf16[64,4,2048]{2,1,0:T(4,128)(2,1)} %bitcast.4) | data formatting | bytes 2097152
where the time goes:
time: 105 us; the launch traced here: 104 us
  Pallas kernels  102 us (97%)
  local copies, waits for them, and re-layouts  2.67 us (3%)
    pallas_call x1, Pallas kernels, body(): pl.pallas_call(functools.partial(kernel, n_sp, n_tp), out_shape=jax.Shape...  102 us
    unnamed x1, local copies, waits for them, and re-layouts  2.67 us

commit v1 on v0

--- a/solution.py
+++ b/solution.py
@@ -38,7 +38,10 @@
     me = lax.axis_index("tp")
 
     def along(step):
-        return lax.rem(z + step + n_sp, n_sp)
+        return z + step
+
+    def exists(step):
+        return (z + step >= 0) if step < 0 else (z + step < n_sp)
 
     def peer(step):
         return lax.rem(me + step, n_tp)
@@ -67,8 +70,16 @@
     gall[pl.ds(me, 1)] = gain[...][None]
 
     barrier = pltpu.get_barrier_semaphore()
+    near = 0
     for step in (-2, -1, 1, 2):
-        pl.semaphore_signal(barrier, inc=1, device_id={"sp": along(step)}, device_id_type=MESH_ID)
+        near = near + exists(step).astype(jnp.int32)
+
+        @pl.when(exists(step))
+        def _():
+            pl.semaphore_signal(
+                barrier, inc=1, device_id={"sp": along(step)}, device_id_type=MESH_ID
+            )
+
     for step in range(1, n_tp):
         pl.semaphore_signal(barrier, inc=1, device_id={"tp": peer(step)}, device_id_type=MESH_ID)
 
@@ -92,11 +103,22 @@
     bias1[...] = log_count((key >= query).astype(jnp.int32) + same)
     bias2[...] = log_count(same)
     bias4[...] = log_count(jnp.where(key >= query, same, 0)) + jnp.where(z >= 1, 0.0, NEGATIVE)
+
+    @pl.when(z < 1)
+    def _():
+        kv_prev[...] = jnp.zeros_like(kv_prev)
+        i_three[...] = jnp.zeros_like(i_three)
+        t_three[...] = jnp.full_like(t_three, NEGATIVE)
+
+    @pl.when(z < 2)
+    def _():
+        i_two[...] = jnp.zeros_like(i_two)
+        t_two[...] = jnp.full_like(t_two, NEGATIVE)
+
     for c in range(CLASSES):
         gap = CLASSES * size + CLASSES * (query - (size - reach + lax.rem(key, reach))) + c - key // reach
         biasc[c] = log_count((gap <= 128).astype(jnp.int32))
 
-    pl.semaphore_wait(barrier, 4 + n_tp - 1)
 
     gains = [
         remote(gall.at[me], gall.at[me], g_ss.at[j - 1], g_rs.at[j - 1], "tp", peer(j))
@@ -106,10 +128,7 @@
         remote(wo, wall.at[me], w_ss.at[j // 2 - 1], w_rs.at[j // 2 - 1], "tp", peer(j))
         for j in range(2, n_tp, 2)
     ]
-    for copy in gains + across:
-        copy.start()
     beside = [remote(wo, wall.at[me], v_ss.at[0], v_rs.at[0], "tp", sibling)]
-    beside[0].start()
 
     def send_q(c):
         return remote(q_own.at[c], q_two.at[c], q_ss.at[c], q_rs.at[c], "sp", along(-2))
@@ -135,8 +154,7 @@
     for copy in weights:
         copy.wait()
 
-    @pl.loop(0, CLASSES)
-    def _(c):
+    def project_class(c):
         tok_copy(c).wait()
         rows = tok[c].reshape(size * batch, tok.shape[3])
         product = jnp.dot(rows, wqkv[...], preferred_element_type=F32)
@@ -147,8 +165,27 @@
             q_own[c, b] = (acc[0, picked, :] * HEAD_DIM ** (-0.5)).astype(BF)
             kv_own[c, b, 0] = acc[1, picked, :].astype(BF)
             kv_own[c, b, 1] = acc[2, picked, :].T.astype(BF)
-        send_q(c).start()
-        send_kv(c).start()
+
+    def send_class(c):
+        @pl.when(exists(-2))
+        def _():
+            send_q(c).start()
+
+        @pl.when(exists(1))
+        def _():
+            send_kv(c).start()
+
+    project_class(0)
+    pl.semaphore_wait(barrier, near + n_tp - 1)
+    send_class(0)
+    for copy in gains + across:
+        copy.start()
+    beside[0].start()
+
+    @pl.loop(1, CLASSES)
+    def _(c):
+        project_class(c)
+        send_class(c)
 
     lane = lax.broadcasted_iota(jnp.int32, (1, LANES), 1)
     head0 = jnp.where(lane < HEAD_DIM, 1.0, 0.0).astype(BF)
@@ -181,9 +218,6 @@
             merged.append((part_a * by_a + part_b * by_b, top, total_a * by_a + total_b * by_b))
         return merged
 
-    def masked(state, valid):
-        return [(part, jnp.where(valid, top, NEGATIVE), total) for part, top, total in state]
-
     def put(part_ref, stat_ref, c, b, state):
         for h in range(2):
             part, top, total = state[h]
@@ -203,8 +237,13 @@
 
     @pl.loop(0, CLASSES)
     def _(c):
-        send_q(c).wait_recv()
-        pass_q(c).start()
+        @pl.when(exists(2))
+        def _():
+            send_q(c).wait_recv()
+
+            @pl.when(exists(-1))
+            def _():
+                pass_q(c).start()
 
         @pl.loop(0, batch)
         def _(b):
@@ -215,53 +254,62 @@
 
     @pl.loop(0, CLASSES)
     def _(c):
-        pass_q(c).wait_recv()
-        send_kv(c).wait_recv()
-        bias = jnp.concatenate([bias2[...], bias4[...]], axis=0)
-        for b in range(batch):
-            keys = jnp.concatenate([kv_own[c, b, 0], kv_prev[c, b, 0]], axis=0)
-            values = jnp.concatenate([kv_own[c, b, 1], kv_prev[c, b, 1]], axis=1)
-            state = masked(attend(q_three[c, b], keys, values, bias), z + 3 < n_sp)
-            put(o_three, s_three, c, b, state)
-        for copy in send_three(c):
-            copy.start()
-
-    @pl.loop(0, CLASSES)
-    def _(c):
-        for copy in send_three(c):
-            copy.wait_recv()
-        for b in range(batch):
-            state = masked(
-                attend(q_two[c, b], kv_own[c, b, 0], kv_own[c, b, 1], bias2[...]), z + 2 < n_sp
-            )
-            put(o_two, s_two, c, b, merge(state, get(i_three, t_three, c, b)))
-        for copy in send_two(c):
-            copy.start()
+        @pl.when(exists(-1))
+        def _():
+            send_kv(c).wait_recv()
+
+        @pl.when(exists(3))
+        def _():
+            pass_q(c).wait_recv()
+            bias = jnp.concatenate([bias2[...], bias4[...]], axis=0)
+            for b in range(batch):
+                keys = jnp.concatenate([kv_own[c, b, 0], kv_prev[c, b, 0]], axis=0)
+                values = jnp.concatenate([kv_own[c, b, 1], kv_prev[c, b, 1]], axis=1)
+                put(o_three, s_three, c, b, attend(q_three[c, b], keys, values, bias))
+            for copy in send_three(c):
+                copy.start()
+
+    @pl.when(exists(2))
+    def _():
+        @pl.loop(0, CLASSES)
+        def _(c):
+            @pl.when(exists(-1))
+            def _():
+                for copy in send_three(c):
+                    copy.wait_recv()
+
+            for b in range(batch):
+                state = attend(q_two[c, b], kv_own[c, b, 0], kv_own[c, b, 1], bias2[...])
+                put(o_two, s_two, c, b, merge(state, get(i_three, t_three, c, b)))
+            for copy in send_two(c):
+                copy.start()
 
     pick_row = lax.broadcasted_iota(jnp.int32, (LANES, LANES), 0)
     pick_col = lax.broadcasted_iota(jnp.int32, (LANES, LANES), 1)
 
-    @pl.loop(0, batch)
-    def _(b):
-        gathered = jnp.zeros((LANES, LANES), F32)
-        for j in range(CLASSES):
-            hot = (pick_row == size - reach + pick_col - j * reach) & (pick_col // reach == j)
-            gathered = gathered + jnp.dot(
-                kv_prev[j, b, 1], jnp.where(hot, 1.0, 0.0).astype(BF), preferred_element_type=F32
-            )
-        corner_v[b] = gathered.astype(BF)
-
-    @pl.loop(0, CLASSES)
-    def _(c):
-        bias = jnp.concatenate([bias1[...], biasc[c]], axis=0)
-        for b in range(batch):
-            keys = jnp.concatenate(
-                [kv_prev[c, b, 0]]
-                + [kv_prev[j, b, 0, size - reach:size, :] for j in range(CLASSES)], axis=0
-            )
-            values = jnp.concatenate([kv_prev[c, b, 1], corner_v[b]], axis=1)
-            state = masked(attend(q_own[c, b], keys, values, bias), z >= 1)
-            put(n_loc, s_loc, c, b, merge(state, get(n_loc, s_loc, c, b)))
+    @pl.when(exists(-1))
+    def _():
+        @pl.loop(0, batch)
+        def _(b):
+            gathered = jnp.zeros((LANES, LANES), F32)
+            for j in range(CLASSES):
+                hot = (pick_row == size - reach + pick_col - j * reach) & (pick_col // reach == j)
+                gathered = gathered + jnp.dot(
+                    kv_prev[j, b, 1], jnp.where(hot, 1.0, 0.0).astype(BF), preferred_element_type=F32
+                )
+            corner_v[b] = gathered.astype(BF)
+
+        @pl.loop(0, CLASSES)
+        def _(c):
+            bias = jnp.concatenate([bias1[...], biasc[c]], axis=0)
+            for b in range(batch):
+                keys = jnp.concatenate(
+                    [kv_prev[c, b, 0]]
+                    + [kv_prev[j, b, 0, size - reach:size, :] for j in range(CLASSES)], axis=0
+                )
+                values = jnp.concatenate([kv_prev[c, b, 1], corner_v[b]], axis=1)
+                state = attend(q_own[c, b], keys, values, bias)
+                put(n_loc, s_loc, c, b, merge(state, get(n_loc, s_loc, c, b)))
 
     for j, copy in enumerate(across):
         copy.wait_recv()
@@ -278,8 +326,11 @@
         )
 
     def finish(c):
-        for copy in send_two(c):
-            copy.wait_recv()
+        @pl.when(exists(-2))
+        def _():
+            for copy in send_two(c):
+                copy.wait_recv()
+
         for b in range(batch):
             state = merge(get(n_loc, s_loc, c, b), get(i_two, t_two, c, b))
             mixed = jnp.concatenate([part / total for part, _, total in state], axis=0)
@@ -328,8 +379,28 @@
 
     @pl.loop(0, CLASSES)
     def _(c):
-        for copy in (send_q(c), pass_q(c), send_kv(c)) + send_three(c) + send_two(c):
-            copy.wait_send()
+        @pl.when(exists(-2))
+        def _():
+            send_q(c).wait_send()
+
+        @pl.when(exists(1))
+        def _():
+            send_kv(c).wait_send()
+
+        @pl.when(exists(2))
+        def _():
+            for copy in send_two(c):
+                copy.wait_send()
+
+            @pl.when(exists(-1))
+            def _():
+                pass_q(c).wait_send()
+
+        @pl.when(exists(3))
+        def _():
+            for copy in send_three(c):
+                copy.wait_send()
+
         for j in range(1, n_tp):
             send_x(c, j).wait_send()
 

time: 105 us -> 86.7 us (0.83)
  the two profiles are of different devices: /device:TPU:33 before, /device:TPU:297 now
where the time goes in v1:
time: 86.7 us; the launch traced here: 86.6 us
  Pallas kernels  83.9 us (97%)
  local copies, waits for them, and re-layouts  2.67 us (3%)
    pallas_call x1, Pallas kernels, body(): pl.pallas_call(functools.partial(kernel, n_sp, n_tp), out_shape=jax.Shape...  83.9 us
    unnamed x1, local copies, waits for them, and re-layouts  2.67 us

profile of v1, /device:TPU:297, one launch (start us, length us, event | category | flops | bytes accessed | tf_op | source)
XLA Modules:
  0.0 86.6 jit_solution(15511446723111748273)
XLA Ops:
  0.0 83.9 %attend_all.1 = bf16[16,4,4,2048]{3,2,1,0:T(4,128)(2,1)} custom-call(bf16[128,4,4,2048]{3,2,1,0:T(4,128)(2,1)} %bitcast.3, bf16[2048,128]{1,0:T(8,128)(2,1)} %wq.1, bf16[2048,128]{1,0:T(8,128)(2,1)} %wk.1, bf16[2048,128]{1,0:T(8,128)(2,1)} %wv.1, f32[1,128]{1,0:T(1,128)} %bitcast.5, bf16[128,2048]{1,0:T(8,128)(2,1)} %wo.1), custom_call_target="tpu_custom_call" | custom-call | tf_op jit(solution)/shard_map/attend_all/pallas_call | solution.py:455
  83.9 2.7 %copy.8 = bf16[64,4,2048]{2,1,0:T(4,128)(2,1)} copy(bf16[64,4,2048]{2,1,0:T(4,128)(2,1)} %bitcast.4) | data formatting | bytes 2097152

commit v2 on v1

--- a/solution.py
+++ b/solution.py
@@ -25,7 +25,7 @@
     o_three, s_three, i_three, t_three, o_two, s_two, i_two, t_two,
     n_loc, s_loc, corner_v, bias0, bias1, biasc, bias2, bias4,
     x_send, x_recv, x_rows,
-    tok_sem, w_sem, own_sem,
+    tok_sem, w_sem, own_sem, in_one, in_two,
     q_ss, q_rs, f_ss, f_rs, k_ss, k_rs,
     o3_ss, o3_rs, t3_ss, t3_rs, o2_ss, o2_rs, t2_ss, t2_rs,
     x_ss, x_rs, g_ss, g_rs, w_ss, w_rs, v_ss, v_rs,
@@ -63,25 +63,110 @@
     ]
     for copy in weights:
         copy.start()
-    for c in range(CLASSES):
-        tok_copy(c).start()
+    tok_copy(0).start()
     own_w = pltpu.make_async_copy(wo, wall.at[me], own_sem)
-    own_w.start()
     gall[pl.ds(me, 1)] = gain[...][None]
 
     barrier = pltpu.get_barrier_semaphore()
     near = 0
-    for step in (-2, -1, 1, 2):
+    for step in (1, 2):
         near = near + exists(step).astype(jnp.int32)
 
-        @pl.when(exists(step))
+        @pl.when(exists(-step))
         def _():
             pl.semaphore_signal(
-                barrier, inc=1, device_id={"sp": along(step)}, device_id_type=MESH_ID
+                barrier, inc=1, device_id={"sp": along(-step)}, device_id_type=MESH_ID
             )
 
     for step in range(1, n_tp):
         pl.semaphore_signal(barrier, inc=1, device_id={"tp": peer(step)}, device_id_type=MESH_ID)
+
+    gains = [
+        remote(gall.at[me], gall.at[me], g_ss.at[j - 1], g_rs.at[j - 1], "tp", peer(j))
+        for j in range(1, n_tp)
+    ]
+    across = [
+        remote(wo, wall.at[me], w_ss.at[j // 2 - 1], w_rs.at[j // 2 - 1], "tp", peer(j))
+        for j in range(2, n_tp, 2)
+    ]
+
+    def handed(j):
+        block = wo if j == 0 else wall.at[peer(n_tp - 2 * j)]
+        place = wall.at[me] if j == 0 else block
+        return remote(block, place, v_ss.at[j], v_rs.at[j], "tp", sibling)
+
+    beside = [handed(j) for j in range(n_tp // 2)]
+
+    def send_q(c):
+        return remote(q_own.at[c], q_two.at[c], q_ss.at[c], q_rs.at[c], "sp", along(-2))
+
+    def pass_q(c):
+        return remote(q_two.at[c], q_three.at[c], f_ss.at[c], f_rs.at[c], "sp", along(-1))
+
+    def send_kv(c):
+        return remote(kv_own.at[c], kv_prev.at[c], k_ss.at[c], k_rs.at[c], "sp", along(1))
+
+    def send_three(c):
+        return (
+            remote(o_three.at[c], i_three.at[c], o3_ss.at[c], o3_rs.at[c], "sp", along(1)),
+            remote(s_three.at[c], t_three.at[c], t3_ss.at[c], t3_rs.at[c], "sp", along(1)),
+        )
+
+    def send_two(c):
+        return (
+            remote(o_two.at[c], i_two.at[c], o2_ss.at[c], o2_rs.at[c], "sp", along(2)),
+            remote(s_two.at[c], t_two.at[c], t2_ss.at[c], t2_rs.at[c], "sp", along(2)),
+        )
+
+    for copy in weights:
+        copy.wait()
+
+    def project_class(c):
+        tok_copy(c).wait()
+
+        @pl.when(c + 1 < CLASSES)
+        def _():
+            tok_copy(c + 1).start()
+
+        rows = tok[c].reshape(size * batch, tok.shape[3])
+        product = jnp.dot(rows, wqkv[...], preferred_element_type=F32)
+        for i in range(3):
+            acc[i] = product[:, i * LANES:(i + 1) * LANES]
+        for b in range(batch):
+            picked = pl.ds(b, size, stride=batch)
+            q_own[c, b] = (acc[0, picked, :] * HEAD_DIM ** (-0.5)).astype(BF)
+            kv_own[c, b, 0] = acc[1, picked, :].astype(BF)
+            kv_own[c, b, 1] = acc[2, picked, :].T.astype(BF)
+
+    def start_q(c):
+        @pl.when(exists(-2))
+        def _():
+            send_q(c).start()
+
+    def start_kv(c):
+        @pl.when(exists(1))
+        def _():
+            send_kv(c).start()
+
+    project_class(jnp.int32(0))
+    own_w.start()
+    pl.semaphore_wait(barrier, near + n_tp - 1)
+    start_kv(0)
+    for step, sem in ((1, in_one), (2, in_two)):
+        @pl.when(exists(step))
+        def _():
+            pl.semaphore_signal(
+                sem, inc=1, device_id={"sp": along(step)}, device_id_type=MESH_ID
+            )
+
+    @pl.when(z > 2)
+    def _():
+        pl.semaphore_wait(in_two, 1)
+        start_q(0)
+
+    for copy in gains + across:
+        copy.start()
+    beside[0].start()
 
     key = lax.broadcasted_iota(jnp.int32, (size, LANES), 0)
     query = lax.broadcasted_iota(jnp.int32, (size, LANES), 1)
@@ -120,72 +205,15 @@
         biasc[c] = log_count((gap <= 128).astype(jnp.int32))
 
 
-    gains = [
-        remote(gall.at[me], gall.at[me], g_ss.at[j - 1], g_rs.at[j - 1], "tp", peer(j))
-        for j in range(1, n_tp)
-    ]
-    across = [
-        remote(wo, wall.at[me], w_ss.at[j // 2 - 1], w_rs.at[j // 2 - 1], "tp", peer(j))
-        for j in range(2, n_tp, 2)
-    ]
-    beside = [remote(wo, wall.at[me], v_ss.at[0], v_rs.at[0], "tp", sibling)]
-
-    def send_q(c):
-        return remote(q_own.at[c], q_two.at[c], q_ss.at[c], q_rs.at[c], "sp", along(-2))
-
-    def pass_q(c):
-        return remote(q_two.at[c], q_three.at[c], f_ss.at[c], f_rs.at[c], "sp", along(-1))
-
-    def send_kv(c):
-        return remote(kv_own.at[c], kv_prev.at[c], k_ss.at[c], k_rs.at[c], "sp", along(1))
-
-    def send_three(c):
-        return (
-            remote(o_three.at[c], i_three.at[c], o3_ss.at[c], o3_rs.at[c], "sp", along(1)),
-            remote(s_three.at[c], t_three.at[c], t3_ss.at[c], t3_rs.at[c], "sp", along(1)),
-        )
-
-    def send_two(c):
-        return (
-            remote(o_two.at[c], i_two.at[c], o2_ss.at[c], o2_rs.at[c], "sp", along(2)),
-            remote(s_two.at[c], t_two.at[c], t2_ss.at[c], t2_rs.at[c], "sp", along(2)),
-        )
-
-    for copy in weights:
-        copy.wait()
-
-    def project_class(c):
-        tok_copy(c).wait()
-        rows = tok[c].reshape(size * batch, tok.shape[3])
-        product = jnp.dot(rows, wqkv[...], preferred_element_type=F32)
-        for i in range(3):
-            acc[i] = product[:, i * LANES:(i + 1) * LANES]
-        for b in range(batch):
-            picked = pl.ds(b, size, stride=batch)
-            q_own[c, b] = (acc[0, picked, :] * HEAD_DIM ** (-0.5)).astype(BF)
-            kv_own[c, b, 0] = acc[1, picked, :].astype(BF)
-            kv_own[c, b, 1] = acc[2, picked, :].T.astype(BF)
-
-    def send_class(c):
-        @pl.when(exists(-2))
-        def _():
-            send_q(c).start()
-
-        @pl.when(exists(1))
-        def _():
-            send_kv(c).start()
-
-    project_class(0)
-    pl.semaphore_wait(barrier, near + n_tp - 1)
-    send_class(0)
-    for copy in gains + across:
-        copy.start()
-    beside[0].start()
-
     @pl.loop(1, CLASSES)
     def _(c):
         project_class(c)
-        send_class(c)
+        start_kv(c)
+
+        @pl.when((c == 1) & (z > 2))
+        def _():
+            start_q(c)
+
 
     lane = lax.broadcasted_iota(jnp.int32, (1, LANES), 1)
     head0 = jnp.where(lane < HEAD_DIM, 1.0, 0.0).astype(BF)
@@ -218,6 +246,22 @@
             merged.append((part_a * by_a + part_b * by_b, top, total_a * by_a + total_b * by_b))
         return merged
 
+    def pack(part_ref, stat_ref, c, b, state):
+        for h in range(2):
+            part, top, total = state[h]
+            part_ref[c, b, h * HEAD_DIM:(h + 1) * HEAD_DIM, :] = (part / total).astype(BF)
+            stat_ref[c, b, h:h + 1, :] = top + jnp.log(total)
+
+    def unpack(part_ref, stat_ref, c, b):
+        return [
+            (
+                part_ref[c, b, h * HEAD_DIM:(h + 1) * HEAD_DIM, :].astype(F32),
+                stat_ref[c, b, h:h + 1, :],
+                jnp.ones((1, LANES), F32),
+            )
+            for h in range(2)
+        ]
+
     def put(part_ref, stat_ref, c, b, state):
         for h in range(2):
             part, top, total = state[h]
@@ -235,16 +279,37 @@
             for h in range(2)
         ]
 
-    @pl.loop(0, CLASSES)
-    def _(c):
+    def three_ahead(c):
+        @pl.when(exists(-1))
+        def _():
+            send_kv(c).wait_recv()
+
+        @pl.when(exists(3))
+        def _():
+            pass_q(c).wait_recv()
+            bias = jnp.concatenate([bias2[...], bias4[...]], axis=0)
+            for b in range(batch):
+                keys = jnp.concatenate([kv_own[c, b, 0], kv_prev[c, b, 0]], axis=0)
+                values = jnp.concatenate([kv_own[c, b, 1], kv_prev[c, b, 1]], axis=1)
+                pack(o_three, s_three, c, b, attend(q_three[c, b], keys, values, bias))
+            for copy in send_three(c):
+                copy.start()
+
+    def two_ahead(c):
         @pl.when(exists(2))
         def _():
-            send_q(c).wait_recv()
-
             @pl.when(exists(-1))
             def _():
-                pass_q(c).start()
-
+                for copy in send_three(c):
+                    copy.wait_recv()
+
+            for b in range(batch):
+                state = attend(q_two[c, b], kv_own[c, b, 0], kv_own[c, b, 1], bias2[...])
+                pack(o_two, s_two, c, b, merge(state, unpack(i_three, t_three, c, b)))
+            for copy in send_two(c):
+                copy.start()
+
+    def own_shard(c):
         @pl.loop(0, batch)
         def _(b):
             keys = jnp.concatenate([kv_own[j, b, 0] for j in range(CLASSES)], axis=0)
@@ -252,37 +317,91 @@
             bias = jnp.concatenate([bias0[c - j + CLASSES - 1] for j in range(CLASSES)], axis=0)
             put(n_loc, s_loc, c, b, attend(q_own[c, b], keys, values, bias))
 
-    @pl.loop(0, CLASSES)
-    def _(c):
-        @pl.when(exists(-1))
-        def _():
-            send_kv(c).wait_recv()
-
-        @pl.when(exists(3))
-        def _():
-            pass_q(c).wait_recv()
-            bias = jnp.concatenate([bias2[...], bias4[...]], axis=0)
-            for b in range(batch):
-                keys = jnp.concatenate([kv_own[c, b, 0], kv_prev[c, b, 0]], axis=0)
-                values = jnp.concatenate([kv_own[c, b, 1], kv_prev[c, b, 1]], axis=1)
-                put(o_three, s_three, c, b, attend(q_three[c, b], keys, values, bias))
-            for copy in send_three(c):
-                copy.start()
-
-    @pl.when(exists(2))
+    def relay(c):
+        @pl.when(exists(2))
+        def _():
+            send_q(c).wait_recv()
+
+            @pl.when(exists(-1))
+            def _():
+                pass_q(c).start()
+
+    @pl.when(z > 0)
     def _():
         @pl.loop(0, CLASSES)
         def _(c):
-            @pl.when(exists(-1))
+            own_shard(c)
+
+            @pl.when(z >= 2)
             def _():
-                for copy in send_three(c):
-                    copy.wait_recv()
-
-            for b in range(batch):
-                state = attend(q_two[c, b], kv_own[c, b, 0], kv_own[c, b, 1], bias2[...])
-                put(o_two, s_two, c, b, merge(state, get(i_three, t_three, c, b)))
-            for copy in send_two(c):
-                copy.start()
+                @pl.when(c == 0)
+                def _():
+                    pl.semaphore_wait(in_one, 1)
+
+                @pl.when(c < 2)
+                def _():
+                    relay(c)
+
+                @pl.when((z == 2) & (c == 1))
+                def _():
+                    pl.semaphore_wait(in_two, 1)
+                    for early in range(CLASSES):
+                        start_q(early)
+
+                @pl.when(c == 3)
+                def _():
+                    relay(2)
+
+            @pl.when(z > 2)
+            def _():
+                @pl.when(c < 2)
+                def _():
+                    start_q(c + 2)
+
+                @pl.when(c >= 2)
+                def _():
+                    three_ahead(c - 2)
+
+    @pl.when(z <= 2)
+    def _():
+        @pl.when(z == 1)
+        def _():
+            pl.semaphore_wait(in_one, 1)
+
+        @pl.loop(0, CLASSES)
+        def _(c):
+            @pl.when((z == 1) | ((z == 2) & (c == 2)))
+            def _():
+                relay(jnp.where(z == 1, c, 3))
+
+            three_ahead(c)
+
+            @pl.when(z == 0)
+            def _():
+                relay(c)
+                two_ahead(c)
+
+        @pl.when(z > 0)
+        def _():
+            @pl.loop(0, CLASSES)
+            def _(c):
+                two_ahead(c)
+
+    @pl.when(z > 2)
+    def _():
+        @pl.loop(0, 2)
+        def _(c):
+            two_ahead(c)
+
+        relay(3)
+
+        @pl.loop(2, CLASSES)
+        def _(c):
+            three_ahead(c)
+
+    for j, copy in enumerate(across):
+        copy.wait_recv()
+        handed(j + 1).start()
 
     pick_row = lax.broadcasted_iota(jnp.int32, (LANES, LANES), 0)
     pick_col = lax.broadcasted_iota(jnp.int32, (LANES, LANES), 1)
@@ -311,11 +430,17 @@
                 state = attend(q_own[c, b], keys, values, bias)
                 put(n_loc, s_loc, c, b, merge(state, get(n_loc, s_loc, c, b)))
 
-    for j, copy in enumerate(across):
-        copy.wait_recv()
-        block = wall.at[peer(n_tp - 2 * (j + 1))]
-        beside.append(remote(block, block, v_ss.at[j + 1], v_rs.at[j + 1], "tp", sibling))
-        beside[-1].start()
+    @pl.when(z > 2)
+    def _():
+        @pl.loop(2, CLASSES)
+        def _(c):
+            two_ahead(c)
+
+    @pl.when(z == 0)
+    def _():
+        @pl.loop(0, CLASSES)
+        def _(c):
+            own_shard(c)
 
     def send_x(c, j):
         to = peer(j)
@@ -332,7 +457,7 @@
                 copy.wait_recv()
 
         for b in range(batch):
-            state = merge(get(n_loc, s_loc, c, b), get(i_two, t_two, c, b))
+            state = merge(get(n_loc, s_loc, c, b), unpack(i_two, t_two, c, b))
             mixed = jnp.concatenate([part / total for part, _, total in state], axis=0)
             x_send[c, b] = mixed.T.astype(BF)
         for j in range(1, n_tp):
@@ -413,7 +538,7 @@
     any_spec = pl.BlockSpec(memory_space=pl.ANY)
     vmem_spec = pl.BlockSpec(memory_space=pltpu.VMEM)
     blocks = (CLASSES, batch, LANES, LANES)
-    stats = (CLASSES, batch, 4, LANES)
+    stats = (CLASSES, batch, 2, LANES)
     dma = pltpu.SemaphoreType.DMA
     tiles = pltpu.VMEM((LANES, LANES), F32)
     scratch = (
@@ -432,7 +557,7 @@
         + [pltpu.VMEM(blocks, BF), pltpu.VMEM(stats, F32)] * 4
         + [
             pltpu.VMEM(blocks, F32),
-            pltpu.VMEM(stats, F32),
+            pltpu.VMEM((CLASSES, batch, 4, LANES), F32),
             pltpu.VMEM((batch, LANES, LANES), BF),
             pltpu.VMEM((2 * CLASSES - 1, LANES, LANES), F32),
             tiles,
@@ -445,6 +570,8 @@
             dma((CLASSES,)),
             dma((3,)),
             dma(()),
+            pltpu.SemaphoreType.REGULAR,
+            pltpu.SemaphoreType.REGULAR,
         ]
         + [dma((CLASSES,))] * 14
         + [dma((CLASSES, n_tp - 1))] * 2

time: 86.7 us -> 87.6 us (1.010)
  the two profiles are of different devices: /device:TPU:297 before, /device:TPU:289 now
where the time goes in v2:
time: 87.6 us; the launch traced here: 87.4 us
  Pallas kernels  84.7 us (97%)
  local copies, waits for them, and re-layouts  2.67 us (3%)
    pallas_call x1, Pallas kernels, body(): pl.pallas_call(functools.partial(kernel, n_sp, n_tp), out_shape=jax.Shape...  84.7 us
    unnamed x1, local copies, waits for them, and re-layouts  2.67 us

profile of v2, /device:TPU:289, one launch (start us, length us, event | category | flops | bytes accessed | tf_op | source)
XLA Modules:
  0.0 87.4 jit_solution(6247447786417873767)
XLA Ops:
  0.0 84.7 %attend_all.1 = bf16[16,4,4,2048]{3,2,1,0:T(4,128)(2,1)} custom-call(bf16[128,4,4,2048]{3,2,1,0:T(4,128)(2,1)} %bitcast.3, bf16[2048,128]{1,0:T(8,128)(2,1)} %wq.1, bf16[2048,128]{1,0:T(8,128)(2,1)} %wk.1, bf16[2048,128]{1,0:T(8,128)(2,1)} %wv.1, f32[1,128]{1,0:T(1,128)} %bitcast.5, bf16[128,2048]{1,0:T(8,128)(2,1)} %wo.1), custom_call_target="tpu_custom_call" | custom-call | tf_op jit(solution)/shard_map/attend_all/pallas_call | solution.py:582
  84.7 2.7 %copy.8 = bf16[64,4,2048]{2,1,0:T(4,128)(2,1)} copy(bf16[64,4,2048]{2,1,0:T(4,128)(2,1)} %bitcast.4) | data formatting | bytes 2097152
